TPU v7x, 32 devices: a whole 2x2x4 slice. The times are simulated.
32 devices in a mesh: grp: 2 (over y), fs: 4 (over z), tp: 4 (over x, core).
Axes of the slice: x: 2, y: 2, z: 4, core: 2. Of those that a mesh axis runs over, the one named last changes fastest.
Arguments:
- tokens: bfloat16 [8192, 2048], P(('grp', 'fs')), parts along dimension 0, may hold values from -6 to 6
- mixer_gain: float32 [2048], replicated, may hold values from 0.1 to 1.9
- outer_weight: float32 [2048, 2048], P('fs', 'tp'), may hold values from -0.125 to 0.125
- inner_weight: float32 [2048, 2048], P('fs', 'tp'), may hold values from -0.125 to 0.125
- value_weight: float32 [2048, 2048], P('fs', 'tp'), may hold values from -0.125 to 0.125
- filter_taps: float32 [3, 2048], P(None, 'tp'), may hold values from -3.5 to 3.5
- mixer_weight: float32 [2048, 2048], P('tp', 'fs'), may hold values from -0.125 to 0.125
- outer_scale: float32 [4, 512], P('tp', 'fs'), may hold values from 0.5 to 2
- inner_scale: float32 [4, 512], P('tp', 'fs'), may hold values from 0.5 to 2
- value_scale: float32 [4, 512], P('tp', 'fs'), may hold values from 0.5 to 2
- mixer_scale: float32 [1, 2048], P(None, 'fs'), may hold values from 0.5 to 2
Outputs:
- layer_out: bfloat16 [8192, 2048], P(('grp', 'fs', 'tp')), parts along dimension 0
There are 2 independent parts, one for each index of `grp`. A program takes and returns all parts, laid end to end along the dimension named above; an argument that names none is the same for every part. Nothing has to cross between parts.
All inputs are finite; a program needn't handle non-finite values.
Results may differ from a plain program's by a relative error of at most 0.014.
Values may be sent and summed in bfloat16 or wider, within the bound.
A program may use at most 64 MiB of HBM per device.

v0:
```python
import jax
import jax.numpy as jnp
from jax import lax
from jax.sharding import PartitionSpec as P

EPS = 1e-06


def normed(rows, gain):
    values = rows.astype(jnp.float32)
    inverse = lax.rsqrt(jnp.mean(values * values, axis=-1, keepdims=True) + EPS)
    return (values * inverse * gain).astype(jnp.bfloat16)


def rounded(values):
    return lax.optimization_barrier(values.astype(jnp.bfloat16)).astype(jnp.float32)


def add_rows(left, piece):
    return jnp.dot(left, piece, preferred_element_type=jnp.float32)


def per_device(
    tokens,
    mixer_gain,
    outer_weight,
    inner_weight,
    value_weight,
    filter_taps,
    mixer_weight,
    outer_scale,
    inner_scale,
    value_scale,
    mixer_scale,
):
    gathered = (
        lax.all_gather(outer_scale, "fs", axis=1, tiled=True),
        lax.all_gather(inner_scale, "fs", axis=1, tiled=True),
        lax.all_gather(value_scale, "fs", axis=1, tiled=True),
        lax.all_gather(mixer_scale, "fs", axis=1, tiled=True),
    )
    outer_col, inner_col, value_col, mixer_col = [piece.reshape(-1) for piece in gathered]
    seq_rows = tokens.shape[0]
    normal_rows = normed(tokens, mixer_gain)

    def fold_one(piece):
        return add_rows(normal_rows, piece)

    outer_sum = fold_one(
        lax.all_gather(outer_weight.astype(jnp.bfloat16), "fs", axis=0, tiled=True)
    )
    inner_sum = fold_one(
        lax.all_gather(inner_weight.astype(jnp.bfloat16), "fs", axis=0, tiled=True)
    )
    value_sum = fold_one(
        lax.all_gather(value_weight.astype(jnp.bfloat16), "fs", axis=0, tiled=True)
    )
    outer = rounded(outer_sum * outer_col)
    inner = rounded(inner_sum * inner_col)
    value = rounded(value_sum * value_col)
    padded = jnp.pad(inner * value, ((2, 0), (0, 0)))
    filtered = (
        filter_taps[0] * padded[0:seq_rows]
        + filter_taps[1] * padded[1 : seq_rows + 1]
        + filter_taps[2] * padded[2:]
    )
    gated = (outer * filtered).astype(jnp.bfloat16)
    mixer_full = lax.all_gather(mixer_weight.astype(jnp.bfloat16), "fs", axis=1, tiled=True)
    return lax.psum_scatter(
        (jnp.dot(gated, mixer_full, preferred_element_type=jnp.float32) * mixer_col).astype(
            jnp.bfloat16
        ),
        "tp",
        scatter_dimension=0,
        tiled=True,
    )


def solution(mesh):
    in_specs = (
        P(("grp", "fs"), None),
        P(),
        P("fs", "tp"),
        P("fs", "tp"),
        P("fs", "tp"),
        P(None, "tp"),
        P("tp", "fs"),
        P("tp", "fs"),
        P("tp", "fs"),
        P("tp", "fs"),
        P(None, "fs"),
    )
    out_specs = P(("grp", "fs", "tp"), None)
    return jax.shard_map(
        per_device, mesh=mesh, in_specs=in_specs, out_specs=out_specs, check_vma=False
    )
```

profile of v0, /device:TPU:0, one launch (start us, length us, event | category | flops | bytes accessed | tf_op | source)
XLA Modules:
  0.0 252.3 jit_solution(7031129598482165264)
XLA Ops:
  6.5 2.2 convert_element_type.46
  8.8 0.0 all-gather.5.cloned.1.call-update
  8.8 0.0 all-gather.7.cloned.1.call-start
  8.9 0.9 convert_element_type.49
  9.8 0.0 all-gather.9.cloned.1.call-start
  9.9 0.9 convert_element_type.52
  10.8 0.0 all-gather.11.cloned.1.call-start
  10.8 0.9 convert_element_type.56
  11.8 0.0 reduce-scatter.2.cloned.1.call-start
  11.8 12.7 %all_gather.25 = f32[1,512]{1,0:T(1,128)S(1)} all-gather(f32[1,128]{1,0:T(1,128)S(1)} %copy-done.5), channel_id=1, replica_groups=mesh['grp'=2,'fs'=4,'tp'=4] {'fs'}, dimensions={1}, use_global_device_ids=true | all-gather | bytes 2560 | tf_op jit(solution)/shard_map/all_gather | solution.py:37
  24.6 7.9 %all_gather.27 = f32[1,512]{1,0:T(1,128)S(1)} all-gather(f32[1,128]{1,0:T(1,128)S(1)} %copy-done.6), channel_id=1, replica_groups=mesh['grp'=2,'fs'=4,'tp'=4] {'fs'}, dimensions={1}, use_global_device_ids=true | all-gather | bytes 2560 | tf_op jit(solution)/shard_map/all_gather | solution.py:38
  32.5 11.0 %all_gather.29 = f32[1,512]{1,0:T(1,128)S(1)} all-gather(f32[1,128]{1,0:T(1,128)S(1)} %copy-done.7), channel_id=1, replica_groups=mesh['grp'=2,'fs'=4,'tp'=4] {'fs'}, dimensions={1}, use_global_device_ids=true | all-gather | bytes 2560 | tf_op jit(solution)/shard_map/all_gather | solution.py:39
  43.5 12.6 %all_gather.31 = f32[1,2048]{1,0:T(1,128)S(1)} all-gather(f32[1,512]{1,0:T(1,128)S(1)} %copy-done.4), channel_id=1, replica_groups=mesh['grp'=2,'fs'=4,'tp'=4] {'fs'}, dimensions={1}, use_global_device_ids=true | all-gather | bytes 10240 | tf_op jit(solution)/shard_map/all_gather | solution.py:40
  56.2 3.1 %fusion = f32[1024]{0:T(1024)S(1)} fusion(bf16[1024,2048]{1,0:T(8,128)(2,1)} %param.11), kind=kLoop, calls=%fused_computation.2 | loop fusion | flops 6290432 | bytes 4198400 | tf_op jit(solution)/shard_map/reduce_sum | solution.py:11
  59.3 0.0 all-gather.5.cloned.1.call-done
  59.4 6.2 %multiply_convert_fusion.4 = bf16[1024,512]{1,0:T(8,128)(2,1)} fusion(bf16[2048,512]{1,0:T(8,128)(2,1)} %all-gather.5.cloned.1.call-done, f32[512]{0:T(512)S(1)} %bitcast.14, bf16[1024,2048]{1,0:T(8,128)(2,1)} %param.11, f32[2048]{0:T(1024)S(1)} %copy-done.8, f32[1024]{0:T(1024)S(1)} %add_rsqrt_fusion), kind=kOutput, calls=%fused_computation.10 | convolution fusion | flops 2156920832 | bytes 7354368 | tf_op jit(solution)/shard_map/dot_general | solution.py:20
  65.6 38.0 %all-gather.7.cloned.1.call-done = bf16[2048,512]{1,0:T(8,128)(2,1)} async-done(((bf16[512,512]{1,0:T(8,128)(2,1)}), bf16[2048,512]{1,0:T(8,128)(2,1)}) %all-gather.7.cloned.1.call-update) | async-done | bytes 2097168 | tf_op jit(solution)/shard_map/all_gather | solution.py:53
  103.6 5.2 %multiply_convert_fusion.3 = bf16[1024,512]{1,0:T(8,128)(2,1)S(1)} fusion(bf16[2048,512]{1,0:T(8,128)(2,1)} %all-gather.7.cloned.1.call-done, f32[512]{0:T(512)S(1)} %bitcast.13, bf16[1024,2048]{1,0:T(8,128)(2,1)} %param.11, f32[2048]{0:T(1024)S(1)} %copy-done.8, f32[1024]{0:T(1024)S(1)} %add_rsqrt_fusion), kind=kOutput, calls=%fused_computation.9 | convolution fusion | flops 2156920832 | bytes 7354368 | tf_op jit(solution)/shard_map/dot_general | solution.py:20
  108.8 40.8 %all-gather.9.cloned.1.call-done = bf16[2048,512]{1,0:T(8,128)(2,1)} async-done(((bf16[512,512]{1,0:T(8,128)(2,1)}), bf16[2048,512]{1,0:T(8,128)(2,1)}) %all-gather.9.cloned.1.call-update) | async-done | bytes 2097168 | tf_op jit(solution)/shard_map/all_gather | solution.py:56
  149.7 5.2 %multiply_convert_fusion.2 = bf16[1024,512]{1,0:T(8,128)(2,1)S(1)} fusion(bf16[2048,512]{1,0:T(8,128)(2,1)} %all-gather.9.cloned.1.call-done, f32[512]{0:T(512)S(1)} %bitcast.12, bf16[1024,2048]{1,0:T(8,128)(2,1)} %param.11, f32[2048]{0:T(1024)S(1)} %copy-done.8, f32[1024]{0:T(1024)S(1)} %add_rsqrt_fusion), kind=kOutput, calls=%fused_computation.8 | convolution fusion | flops 2156920832 | bytes 7354368 | tf_op jit(solution)/shard_map/dot_general | solution.py:20
  154.9 0.3 convert_multiply_fusion.2
  155.2 40.4 %all-gather.11.cloned.1.call-done = bf16[512,2048]{1,0:T(8,128)(2,1)} async-done(((bf16[512,512]{1,0:T(8,128)(2,1)}), bf16[512,2048]{1,0:T(8,128)(2,1)}) %all-gather.11.cloned.1.call-update) | async-done | bytes 2097168 | tf_op jit(solution)/shard_map/all_gather | solution.py:68
  195.6 6.6 %multiply_convert_fusion = bf16[1024,2048]{1,0:T(8,128)(2,1)} fusion(bf16[512,2048]{1,0:T(8,128)(2,1)} %all-gather.11.cloned.1.call-done, f32[2048]{0:T(1024)S(1)} %bitcast.11, f32[1024,512]{1,0:T(8,128)S(1)} %convert_multiply_fusion.2, bf16[1024,512]{1,0:T(8,128)(2,1)} %multiply_convert_fusion.4, f32[512]{0:T(512)S(1)} %bitcast.16, f32[512]{0:T(512)S(1)} %bitcast.17, ...), kind=kOutput, calls=%fused_computation.5 | convolution fusion | flops 2155872256 | bytes 9451520 | tf_op jit(solution)/shard_map/dot_general | solution.py:70
  202.2 43.6 %reduce-scatter.2.cloned.1.call-done = bf16[256,2048]{1,0:T(8,128)(2,1)} async-done(((bf16[1024,2048]{1,0:T(8,128)(2,1)}), bf16[256,2048]{1,0:T(8,128)(2,1)}) %reduce-scatter.2.cloned.1.call-update) | async-done | bytes 1048592 | tf_op jit(solution)/shard_map/reduce_scatter | solution.py:69
  (25 shorter events, 0.1 us)
Async XLA Ops:
  6.5 2.3 copy-start
  6.5 3.3 %copy-start.1 = (f32[512,512]{1,0:T(8,128)S(1)}, f32[512,512]{1,0:T(8,128)}, u32[]{:S(2)}) copy-start(f32[512,512]{1,0:T(8,128)} %param.15) | copy-start | bytes 3145732
  6.5 52.8 %all-gather.5.cloned.1.call-start = ((), (), s32[]{:S(2)}) async-start(), calls=%async_computation.1 | async-start | bytes 2621440 | tf_op jit(solution)/shard_map/all_gather | solution.py:50
  8.8 2.0 copy-start.2
  8.8 94.8 %all-gather.7.cloned.1.call-start = ((), (), s32[]{:S(2)}) async-start(), calls=%async_computation.2 | async-start | bytes 2621440 | tf_op jit(solution)/shard_map/all_gather | solution.py:53
  9.8 2.1 copy-start.5
  9.8 14.8 %copy-start.6 = (f32[1,128]{1,0:T(1,128)S(1)}, f32[1,128]{1,0:T(1,128)}, u32[]{:S(2)}) copy-start(f32[1,128]{1,0:T(1,128)} %param.19) | copy-start | bytes 1540
  9.8 22.7 %copy-start.7 = (f32[1,128]{1,0:T(1,128)S(1)}, f32[1,128]{1,0:T(1,128)}, u32[]{:S(2)}) copy-start(f32[1,128]{1,0:T(1,128)} %param.20) | copy-start | bytes 1540
  9.8 33.7 %copy-start.4 = (f32[1,512]{1,0:T(1,128)S(1)}, f32[1,512]{1,0:T(1,128)}, u32[]{:S(2)}) copy-start(f32[1,512]{1,0:T(1,128)} %param.21) | copy-start | bytes 6148
  9.8 139.9 %all-gather.9.cloned.1.call-start = ((), (), s32[]{:S(2)}) async-start(), calls=%async_computation.3 | async-start | bytes 2621440 | tf_op jit(solution)/shard_map/all_gather | solution.py:56
  10.8 184.8 %all-gather.11.cloned.1.call-start = ((), (), s32[]{:S(2)}) async-start(), calls=%async_computation.4 | async-start | bytes 2621440 | tf_op jit(solution)/shard_map/all_gather | solution.py:68
  11.8 234.0 %reduce-scatter.2.cloned.1.call-start = ((), (), s32[]{:S(2)}) async-start(), calls=%async_computation.5 | async-start | bytes 5242880 | tf_op jit(solution)/shard_map/reduce_scatter | solution.py:69
  56.2 3.1 %copy-start.3 = (f32[3,512]{1,0:T(4,128)S(1)}, f32[3,512]{1,0:T(4,128)}, u32[]{:S(2)}) copy-start(f32[3,512]{1,0:T(4,128)} %param.16) | copy-start | bytes 18436
  56.2 3.2 %copy-start.8 = (f32[2048]{0:T(1024)S(1)}, f32[2048]{0:T(1024)}, u32[]{:S(2)}) copy-start(f32[2048]{0:T(1024)} %param.12) | copy-start | bytes 24580
Sparse Core Ops, SparseCore 0:
  8.9 48.5 all-gather.4
  59.1 44.4 all-gather.6
  105.2 44.4 all-gather.8
  151.1 44.4 all-gather.10
  202.3 43.3 reduce-scatter.1
where the time goes:
time: 252 us
  waiting for transfers between devices  163 us (65%)
  blocking collectives  44.3 us (18%)
  matrix products  23.3 us (9%)
  between operations  13.3 us (5%)
  other arithmetic  8.31 us (3%)
    reduce_scatter x1, waiting for transfers between devices, per_device(): lax.psum_scatter((jnp.dot(gated, mixer_full, preferred_element_type=jnp.f...  43.6 us
    all_gather x1, waiting for transfers between devices, per_device(): lax.all_gather(value_weight.astype(jnp.bfloat16), 'fs', axis=0, tiled=True)  40.8 us
    all_gather x1, waiting for transfers between devices, per_device(): lax.all_gather(mixer_weight.astype(jnp.bfloat16), 'fs', axis=1, tiled=True)  40.4 us
    all_gather x1, waiting for transfers between devices, per_device(): lax.all_gather(inner_weight.astype(jnp.bfloat16), 'fs', axis=0, tiled=True)  38 us
    dot_general x3, matrix products, add_rows(): return jnp.dot(left, piece, preferred_element_type=jnp.float32)  16.7 us
    all_gather x1, blocking collectives, per_device(): lax.all_gather(outer_scale, 'fs', axis=1, tiled=True)  12.7 us
    all_gather x1, blocking collectives, per_device(): lax.all_gather(mixer_scale, 'fs', axis=1, tiled=True)  12.6 us
    all_gather x1, blocking collectives, per_device(): lax.all_gather(value_scale, 'fs', axis=1, tiled=True)  11 us
  transfers between devices with their start and end apart: 5, of which 4 were waited for; matrix products, arithmetic and copies ran while one was open for 9% of the time, Pallas kernels for 0%

commit v1 on v0

--- a/solution.py
+++ b/solution.py
@@ -50,7 +50,12 @@
         lax.all_gather(outer_weight.astype(jnp.bfloat16), "fs", axis=0, tiled=True)
     )
     inner_sum = fold_one(
-        lax.all_gather(inner_weight.astype(jnp.bfloat16), "fs", axis=0, tiled=True)
+        jnp.concatenate(
+            lax.all_to_all(
+                jnp.stack([inner_weight.astype(jnp.bfloat16)] * lax.axis_size("fs")), "fs", 0, 0
+            ),
+            axis=0,
+        )
     )
     value_sum = fold_one(
         lax.all_gather(value_weight.astype(jnp.bfloat16), "fs", axis=0, tiled=True)

time: 252 us -> 246 us (0.976)
  waiting for transfers between devices: 163 us -> 81.4 us
  blocking collectives: 44.3 us -> 113 us
  starting transfers between devices: 0.17 us -> 6.6 us
    all_gather x1, blocking collectives: 12.7 us -> 71.6 us  [per_device(): lax.all_gather(outer_scale, 'fs', axis=1, tiled=True)]
    all_gather x1, waiting for transfers between devices: 40.8 us -> 1.99 us  [per_device(): lax.all_gather(value_weight.astype(jnp.bfloat16), 'fs', axis=0, tiled=True)]
    all_gather x1 -> x0, waiting for transfers between devices: 38 us -> none  [per_device(): lax.all_gather(inner_weight.astype(jnp.bfloat16), 'fs', axis=0, tiled=True)]
    all_gather x1, blocking collectives: 7.94 us -> 20.4 us  [per_device(): lax.all_gather(inner_scale, 'fs', axis=1, tiled=True)]
    all_to_all x0 -> x1, starting transfers between devices: none -> 6.48 us  [per_device(): lax.all_to_all(jnp.stack([inner_weight.astype(jnp.bfloat16)] * lax.axis_s...]
    all_gather x1, waiting for transfers between devices: 40.4 us -> 35.8 us  [per_device(): lax.all_gather(mixer_weight.astype(jnp.bfloat16), 'fs', axis=1, tiled=True)]
    all_gather x1, blocking collectives: 11 us -> 8.04 us  [per_device(): lax.all_gather(value_scale, 'fs', axis=1, tiled=True)]
  transfers between devices with their start and end apart: 5 -> 5, of which waited for: 4 -> 3; matrix products, arithmetic and copies ran while one was open for 9% -> 9% of each run, Pallas kernels for 0% -> 0%
where the time goes in v1:
time: 246 us
  blocking collectives  113 us (46%)
  waiting for transfers between devices  81.4 us (33%)
  matrix products  22.8 us (9%)
  between operations  13.2 us (5%)
  other arithmetic  7.53 us (3%)
  starting transfers between devices  6.6 us (3%)
    all_gather x1, blocking collectives, per_device(): lax.all_gather(outer_scale, 'fs', axis=1, tiled=True)  71.6 us
    reduce_scatter x1, waiting for transfers between devices, per_device(): lax.psum_scatter((jnp.dot(gated, mixer_full, preferred_element_type=jnp.f...  43.5 us
    all_gather x1, waiting for transfers between devices, per_device(): lax.all_gather(mixer_weight.astype(jnp.bfloat16), 'fs', axis=1, tiled=True)  35.8 us
    all_gather x1, blocking collectives, per_device(): lax.all_gather(inner_scale, 'fs', axis=1, tiled=True)  20.4 us
    dot_general x3, matrix products, add_rows(): return jnp.dot(left, piece, preferred_element_type=jnp.float32)  16.2 us
    all_gather x1, blocking collectives, per_device(): lax.all_gather(mixer_scale, 'fs', axis=1, tiled=True)  12.6 us
    all_gather x1, blocking collectives, per_device(): lax.all_gather(value_scale, 'fs', axis=1, tiled=True)  8.04 us
    dot_general x1, matrix products, per_device(): jnp.dot(gated, mixer_full, preferred_element_type=jnp.float32) * mixer_col  6.6 us
  transfers between devices with their start and end apart: 5, of which 3 were waited for; matrix products, arithmetic and copies ran while one was open for 9% of the time, Pallas kernels for 0%

profile of v1, /device:TPU:0, one launch (start us, length us, event | category | flops | bytes accessed | tf_op | source)
XLA Modules:
  0.0 245.8 jit_solution(1600985459476163786)
XLA Ops:
  6.5 2.2 convert_element_type.46
  8.8 0.0 all-gather.4.cloned.1.call-update
  8.8 0.0 all-gather.6.cloned.1.call-start
  8.9 0.9 convert_element_type.52
  9.8 0.1 convert_element_type.49
  9.8 1.5 stack.2
  11.4 6.5 %all-to-all-start = ((bf16[4,512,512]{2,1,0:T(8,128)(2,1)}), bf16[4,512,512]{2,1,0:T(8,128)(2,1)S(1)}, u32[]{:S(2)}, u32[]{:S(2)}) async-start(bf16[4,512,512]{2,1,0:T(8,128)(2,1)} %stack.2), calls=%async_computation | async-start | bytes 4194304 | tf_op jit(solution)/shard_map/all_to_all | solution.py:54
  17.9 0.0 all-gather.8.cloned.1.call-start
  17.9 0.9 convert_element_type.56
  18.9 0.0 reduce-scatter.2.cloned.1.call-start
  18.9 71.6 %all_gather.22 = f32[1,512]{1,0:T(1,128)S(1)} all-gather(f32[1,128]{1,0:T(1,128)S(1)} %copy-done.5), channel_id=1, replica_groups=mesh['grp'=2,'fs'=4,'tp'=4] {'fs'}, dimensions={1}, use_global_device_ids=true | all-gather | bytes 2560 | tf_op jit(solution)/shard_map/all_gather | solution.py:37
  90.5 20.4 %all_gather.23 = f32[1,512]{1,0:T(1,128)S(1)} all-gather(f32[1,128]{1,0:T(1,128)S(1)} %copy-done.6), channel_id=1, replica_groups=mesh['grp'=2,'fs'=4,'tp'=4] {'fs'}, dimensions={1}, use_global_device_ids=true | all-gather | bytes 2560 | tf_op jit(solution)/shard_map/all_gather | solution.py:38
  110.9 8.0 %all_gather.25 = f32[1,512]{1,0:T(1,128)S(1)} all-gather(f32[1,128]{1,0:T(1,128)S(1)} %copy-done.7), channel_id=1, replica_groups=mesh['grp'=2,'fs'=4,'tp'=4] {'fs'}, dimensions={1}, use_global_device_ids=true | all-gather | bytes 2560 | tf_op jit(solution)/shard_map/all_gather | solution.py:39
  118.9 12.6 %all_gather.27 = f32[1,2048]{1,0:T(1,128)S(1)} all-gather(f32[1,512]{1,0:T(1,128)S(1)} %copy-done.4), channel_id=1, replica_groups=mesh['grp'=2,'fs'=4,'tp'=4] {'fs'}, dimensions={1}, use_global_device_ids=true | all-gather | bytes 10240 | tf_op jit(solution)/shard_map/all_gather | solution.py:40
  131.6 3.1 %fusion = f32[1024]{0:T(1024)S(1)} fusion(bf16[1024,2048]{1,0:T(8,128)(2,1)} %param.11), kind=kLoop, calls=%fused_computation.2 | loop fusion | flops 6290432 | bytes 4198400 | tf_op jit(solution)/shard_map/reduce_sum | solution.py:11
  134.8 0.0 all-gather.4.cloned.1.call-done
  134.8 6.2 %multiply_convert_fusion.4 = bf16[1024,512]{1,0:T(8,128)(2,1)} fusion(bf16[2048,512]{1,0:T(8,128)(2,1)} %all-gather.4.cloned.1.call-done, f32[512]{0:T(512)S(1)} %bitcast.16, bf16[1024,2048]{1,0:T(8,128)(2,1)} %param.11, f32[2048]{0:T(1024)S(1)} %copy-done.8, f32[1024]{0:T(1024)S(1)} %add_rsqrt_fusion), kind=kOutput, calls=%fused_computation.10 | convolution fusion | flops 2156920832 | bytes 7354368 | tf_op jit(solution)/shard_map/dot_general | solution.py:20
  141.0 2.0 all-gather.6.cloned.1.call-done
  143.0 5.3 %multiply_convert_fusion.2 = bf16[1024,512]{1,0:T(8,128)(2,1)S(1)} fusion(bf16[2048,512]{1,0:T(8,128)(2,1)} %all-gather.6.cloned.1.call-done, f32[512]{0:T(512)S(1)} %bitcast.15, bf16[1024,2048]{1,0:T(8,128)(2,1)} %param.11, f32[2048]{0:T(1024)S(1)} %copy-done.8, f32[1024]{0:T(1024)S(1)} %add_rsqrt_fusion), kind=kOutput, calls=%fused_computation.8 | convolution fusion | flops 2156920832 | bytes 7354368 | tf_op jit(solution)/shard_map/dot_general | solution.py:20
  148.3 4.7 %multiply_convert_fusion.3 = bf16[1024,512]{1,0:T(8,128)(2,1)S(1)} fusion(bf16[2048,512]{1,0:T(8,128)(2,1)S(1)} %bitcast.12, f32[512]{0:T(512)S(1)} %bitcast.14, bf16[1024,2048]{1,0:T(8,128)(2,1)} %param.11, f32[2048]{0:T(1024)S(1)} %copy-done.8, f32[1024]{0:T(1024)S(1)} %add_rsqrt_fusion), kind=kOutput, calls=%fused_computation.9 | convolution fusion | flops 2156920832 | bytes 7354368 | tf_op jit(solution)/shard_map/dot_general | solution.py:20
  153.0 0.3 convert_multiply_fusion.2
  153.3 35.8 %all-gather.8.cloned.1.call-done = bf16[512,2048]{1,0:T(8,128)(2,1)} async-done(((bf16[512,512]{1,0:T(8,128)(2,1)}), bf16[512,2048]{1,0:T(8,128)(2,1)}) %all-gather.8.cloned.1.call-update) | async-done | bytes 2097168 | tf_op jit(solution)/shard_map/all_gather | solution.py:73
  189.1 6.6 %multiply_convert_fusion = bf16[1024,2048]{1,0:T(8,128)(2,1)} fusion(bf16[512,2048]{1,0:T(8,128)(2,1)} %all-gather.8.cloned.1.call-done, f32[2048]{0:T(1024)S(1)} %bitcast.13, f32[1024,512]{1,0:T(8,128)S(1)} %convert_multiply_fusion.2, bf16[1024,512]{1,0:T(8,128)(2,1)} %multiply_convert_fusion.4, f32[512]{0:T(512)S(1)} %bitcast.18, f32[512]{0:T(512)S(1)} %bitcast.19, ...), kind=kOutput, calls=%fused_computation.5 | convolution fusion | flops 2155872256 | bytes 9451520 | tf_op jit(solution)/shard_map/dot_general | solution.py:75
  195.7 43.5 %reduce-scatter.2.cloned.1.call-done = bf16[256,2048]{1,0:T(8,128)(2,1)} async-done(((bf16[1024,2048]{1,0:T(8,128)(2,1)}), bf16[256,2048]{1,0:T(8,128)(2,1)}) %reduce-scatter.2.cloned.1.call-update) | async-done | bytes 1048592 | tf_op jit(solution)/shard_map/reduce_scatter | solution.py:74
  (25 shorter events, 0.1 us)
Async XLA Ops:
  6.5 2.3 copy-start
  6.5 3.2 %copy-start.1 = (f32[512,512]{1,0:T(8,128)S(1)}, f32[512,512]{1,0:T(8,128)}, u32[]{:S(2)}) copy-start(f32[512,512]{1,0:T(8,128)} %param.14) | copy-start | bytes 3145732
  6.5 128.2 %all-gather.4.cloned.1.call-start = ((), (), s32[]{:S(2)}) async-start(), calls=%async_computation.2 | async-start | bytes 2621440 | tf_op jit(solution)/shard_map/all_gather | solution.py:50
  8.8 134.2 %all-gather.6.cloned.1.call-start = ((), (), s32[]{:S(2)}) async-start(), calls=%async_computation.3 | async-start | bytes 2621440 | tf_op jit(solution)/shard_map/all_gather | solution.py:61
  11.4 6.6 %copy-start.2 = (f32[512,512]{1,0:T(8,128)S(1)}, f32[512,512]{1,0:T(8,128)}, u32[]{:S(2)}) copy-start(f32[512,512]{1,0:T(8,128)} %param.17) | copy-start | bytes 3145732
  11.4 136.9 %all-to-all-start = ((bf16[4,512,512]{2,1,0:T(8,128)(2,1)}), bf16[4,512,512]{2,1,0:T(8,128)(2,1)S(1)}, u32[]{:S(2)}, u32[]{:S(2)}) async-start(bf16[4,512,512]{2,1,0:T(8,128)(2,1)} %stack.2), calls=%async_computation | async-start | bytes 4194304 | tf_op jit(solution)/shard_map/all_to_all | solution.py:54
  17.8 1.1 copy-start.5
  17.8 72.7 %copy-start.6 = (f32[1,128]{1,0:T(1,128)S(1)}, f32[1,128]{1,0:T(1,128)}, u32[]{:S(2)}) copy-start(f32[1,128]{1,0:T(1,128)} %param.19) | copy-start | bytes 1540
  17.9 93.1 %copy-start.7 = (f32[1,128]{1,0:T(1,128)S(1)}, f32[1,128]{1,0:T(1,128)}, u32[]{:S(2)}) copy-start(f32[1,128]{1,0:T(1,128)} %param.20) | copy-start | bytes 1540
  17.9 101.1 %copy-start.4 = (f32[1,512]{1,0:T(1,128)S(1)}, f32[1,512]{1,0:T(1,128)}, u32[]{:S(2)}) copy-start(f32[1,512]{1,0:T(1,128)} %param.21) | copy-start | bytes 6148
  17.9 171.2 %all-gather.8.cloned.1.call-start = ((), (), s32[]{:S(2)}) async-start(), calls=%async_computation.4 | async-start | bytes 2621440 | tf_op jit(solution)/shard_map/all_gather | solution.py:73
  18.9 220.4 %reduce-scatter.2.cloned.1.call-start = ((), (), s32[]{:S(2)}) async-start(), calls=%async_computation.5 | async-start | bytes 5242880 | tf_op jit(solution)/shard_map/reduce_scatter | solution.py:74
  131.6 3.1 %copy-start.3 = (f32[3,512]{1,0:T(4,128)S(1)}, f32[3,512]{1,0:T(4,128)}, u32[]{:S(2)}) copy-start(f32[3,512]{1,0:T(4,128)} %param.16) | copy-start | bytes 18436
  131.6 3.2 %copy-start.8 = (f32[2048]{0:T(1024)S(1)}, f32[2048]{0:T(1024)}, u32[]{:S(2)}) copy-start(f32[2048]{0:T(1024)} %param.12) | copy-start | bytes 24580
Sparse Core Ops, SparseCore 0:
  8.9 86.5 all-gather.3
  97.0 45.9 all-gather.5
  144.6 44.4 all-gather.7
  195.8 43.3 reduce-scatter.1
